TPU v7x, 256 devices: a whole 4x4x8 slice. The times are simulated.
256 devices in a mesh: rep: 2 (over z_hi), fs: 16 (over z_lo, y), tp: 8 (over x, core).
Axes of the slice: x: 4, y: 4, z: 8 (z_hi: 2, z_lo: 4; z = z_hi * 4 + z_lo), core: 2. Of those that a mesh axis runs over, the one named last changes fastest.
Arguments:
- stream: bfloat16 [32, 1024, 2048], P(('rep', 'fs'), None, 'tp'), may hold values from -6 to 6
- norm_gain: float32 [2048], replicated, may hold values from 0.1 to 1.9
- w_in: float32 [2048, 512], P('fs', 'tp'), may hold values from -0.125 to 0.125
- s_in: float32 [512], P(('tp', 'fs')), may hold values from 0.1 to 1.9
- pool_w: bfloat16 [4, 128, 128], replicated, may hold values from -0.5 to 0.5
- w_out: float32 [512, 2048], P('fs', 'tp'), may hold values from -0.25 to 0.25
- s_out: float32 [2048], P(('tp', 'fs')), may hold values from 0.1 to 1.9
- ffn_gain: float32 [2048], replicated, may hold values from 0.1 to 1.9
- w_up: float32 [2048, 8192], P('fs', 'tp'), may hold values from -0.125 to 0.125
- s_up: float32 [8192], P(('tp', 'fs')), may hold values from 0.1 to 1.9
- w_down: float32 [8192, 2048], P('tp', 'fs'), may hold values from -0.0625 to 0.0625
- s_down: float32 [2048], P('fs'), may hold values from 0.1 to 1.9
Outputs:
- result: bfloat16 [32, 1024, 2048], P(('rep', 'fs'), None, 'tp')
All inputs are finite; a program needn't handle non-finite values.
Results may differ from a plain program's by a relative error of at most 0.012.
Values may be sent and summed in bfloat16 or wider, within the bound.
No kernel may reach another device: no remote copies, remote signals or barrier semaphores. Data moves between devices by JAX's collectives and lax.ppermute only.
A program may use at most 64 MiB of HBM per device.

v0:
```python
import jax
import jax.numpy as jnp
from jax import lax
from jax.sharding import Mesh
from jax.sharding import PartitionSpec as P

PW = 512
GROUP = 128
FS = ("fs_0", "fs_1")
REP_FS = ("rep", "fs_0", "fs_1")
TP_FS = ("tp", "fs_0", "fs_1")
epsilon = 0.25


def laid_out(parts, dim):
    parts = jnp.moveaxis(parts, 0, dim)
    lengths = parts.shape
    return parts.reshape(*lengths[:dim], lengths[dim] * lengths[dim + 1], *lengths[dim + 2 :])


def gather_packed(arrays, axis, dims):
    ravelled = jnp.concatenate([a.reshape(-1) for a in arrays])
    lines, at, finished = (lax.all_gather(ravelled, axis), 0, [])
    for a, dim in zip(arrays, dims):
        parts = lines[:, at : at + a.size].reshape(-1, *a.shape)
        finished.append(laid_out(parts, dim))
        at += a.size
    return tuple(finished)


def sent_to_all(array, axis):
    count = lax.axis_size(axis)
    return lax.all_to_all(
        jnp.broadcast_to(array[None], (count, *array.shape)), axis, 0, 0, tiled=True
    )


def collect(array, axis, dim):
    return laid_out(sent_to_all(array, axis), dim)


def stacked_from(array, axes, turns):
    parts = array
    for k in turns:
        parts = lax.all_gather(parts, axes[k])
    done = turns[::-1]
    back = [done.index(k) for k in range(len(axes))]
    parts = parts.transpose(*back, *range(len(axes), parts.ndim))
    return parts.reshape(-1, *array.shape)


def whole_of(array, axes, turns, dim):
    return laid_out(stacked_from(array, axes, turns), dim)


def cut_along(array, dim, count):
    lengths = array.shape
    parts = array.reshape(*lengths[:dim], count, lengths[dim] // count, *lengths[dim + 1 :])
    return jnp.moveaxis(parts, dim, 0)


def sent_and_summed(array, axis, dim):
    count = lax.axis_size(axis)
    parts = lax.all_to_all(cut_along(array, dim, count), axis, 0, 0, tiled=True)
    return jnp.sum(parts.astype(jnp.float32), axis=0)


def rms_rows(values, gain):
    floats = values.astype(jnp.float32)
    scale = lax.rsqrt(jnp.mean(floats * floats, axis=-1, keepdims=True) + epsilon)
    return (floats * scale * gain).astype(jnp.bfloat16)


def pool_local(pool_in, first):
    length, width = pool_in.shape
    positions = jnp.arange(length, dtype=jnp.int32)
    source = positions[None, :]
    target = positions[:, None]
    group_of = (first + jnp.arange(width, dtype=jnp.int32)) // GROUP
    means = jnp.zeros((length, width), jnp.float32)
    for level in range(4):
        half = 2**level
        band_ones = ((source >= target - half) & (source < target + half)).astype(jnp.bfloat16)
        counts = (jnp.minimum(positions + half, length) - jnp.maximum(positions - half, 0)).astype(
            jnp.float32
        )
        sums = jnp.dot(band_ones, pool_in, preferred_element_type=jnp.float32) / counts[:, None]
        means = jnp.where(group_of[None, :] == level, sums, means)
    return (means - pool_in.astype(jnp.float32)).astype(jnp.bfloat16)


def fold_rows(left, piece):
    return jnp.dot(left, piece, preferred_element_type=jnp.float32)


def on_device(
    stream, norm_gain, w_in, s_in, pool_w, w_out, s_out, ffn_gain, w_up, s_up, w_down, s_down
):
    tokens = stream[0]
    length = tokens.shape[0]
    scale_in, scale_out, scale_up, scale_down = gather_packed(
        (s_in, s_out, s_up, s_down), FS, (0, 0, 0, 0)
    )
    in_whole, out_whole = gather_packed(
        (w_in.astype(jnp.bfloat16), w_out.astype(jnp.bfloat16)), FS, (0, 0)
    )
    full_rows = lax.all_gather(tokens, "tp", axis=1, tiled=True)
    normed = rms_rows(full_rows, norm_gain)
    projected = jnp.dot(normed, in_whole, preferred_element_type=jnp.float32)
    pool_in = (projected * scale_in).astype(jnp.bfloat16)
    pooled = pool_local(pool_in, lax.axis_index("tp") * pool_in.shape[1])
    pooled_all = collect(pooled, "tp", 1)
    grouped = jnp.einsum(
        "lgc,gcd->lgd",
        pooled_all.reshape(length, 4, GROUP),
        pool_w,
        preferred_element_type=jnp.float32,
    )
    grouped = grouped.reshape(length, PW).astype(jnp.bfloat16)
    branch = jnp.dot(grouped, out_whole, preferred_element_type=jnp.float32)
    mixed = (tokens.astype(jnp.float32) + branch * scale_out).astype(jnp.bfloat16)
    mixed_full = lax.all_gather(mixed, "tp", axis=1, tiled=True)
    ffn_in = rms_rows(mixed_full, ffn_gain)
    upward = fold_rows(ffn_in, whole_of(w_up.astype(jnp.bfloat16), FS, (0, 1), 0))
    hidden = jnp.square(jax.nn.relu(upward * scale_up)).astype(jnp.bfloat16)
    partial_value = jnp.dot(
        hidden,
        whole_of(w_down.astype(jnp.bfloat16), FS, (0, 1), 1),
        preferred_element_type=jnp.float32,
    )
    rounded = lax.optimization_barrier((partial_value * scale_down).astype(jnp.bfloat16))
    summed = sent_and_summed(rounded.astype(jnp.float32).astype(jnp.bfloat16), "tp", 1)
    return (mixed.astype(jnp.float32) + summed).astype(jnp.bfloat16)[None]


def solution(mesh):
    finer = Mesh(
        mesh.devices.reshape(mesh.shape["rep"], 4, 4, mesh.shape["tp"]),
        ("rep", "fs_0", "fs_1", "tp"),
    )
    return jax.shard_map(
        on_device,
        mesh=finer,
        in_specs=(
            P(REP_FS, None, "tp"),
            P(),
            P(FS, "tp"),
            P(TP_FS),
            P(),
            P(FS, "tp"),
            P(TP_FS),
            P(),
            P(FS, "tp"),
            P(TP_FS),
            P("tp", FS),
            P(FS),
        ),
        out_specs=P(REP_FS, None, "tp"),
        check_vma=False,
    )
```

profile of v0, /device:TPU:1, one launch (start us, length us, event | category | flops | bytes accessed | tf_op | source)
XLA Modules:
  0.0 350.2 jit_solution(10267729505535979363)
XLA Ops:
  6.5 1.8 convert_element_type.116
  8.4 0.0 all-gather.22.cloned.1.call-start
  8.4 1.8 convert_element_type.118
  10.2 0.0 all-gather.16.cloned.1.call-start
  10.3 0.7 all-gather.16.cloned.1.call-update
  11.0 34.7 %all-gather.18.cloned.1.call-done = bf16[512,1024]{1,0:T(8,128)(2,1)} async-done(((bf16[128,1024]{1,0:T(8,128)(2,1)}), bf16[512,1024]{1,0:T(8,128)(2,1)}) %all-gather.18.cloned.1.call-update) | async-done | bytes 1048592 | tf_op jit(solution)/shard_map/all_gather | solution.py:45
  45.8 0.8 convert_element_type.100
  46.6 0.1 copy.25
  46.7 0.1 reshape.137
  46.8 0.8 convert_bitcast_fusion
  47.6 1.3 dynamic-slice
  49.6 0.9 maximum_dynamic-update-slice_fusion
  50.5 64.0 %all-reduce = f32[3392]{0:T(1024)S(1)} all-reduce(f32[3392]{0:T(1024)S(1)} %maximum_dynamic-update-slice_fusion), channel_id=4, replica_groups=mesh['rep'=2,'fs_0'=4,'fs_1'=4,'tp'=8] {'fs_0','fs_1'}, use_global_device_ids=true, to_apply=%add | all-reduce | flops 3392 | bytes 27136
  114.5 0.1 reshape.144
  114.6 0.1 mul.87
  114.7 33.1 %all-gather.1 = bf16[262144]{0:T(1024)(128)(2,1)S(1)} all-gather(bf16[16384]{0:T(1024)(128)(2,1)S(1)} %pad_maximum_fusion), channel_id=3, replica_groups=mesh['rep'=2,'fs_0'=4,'fs_1'=4,'tp'=8] {'fs_0','fs_1'}, dimensions={0}, use_global_device_ids=true | all-gather | bytes 557056 | tf_op jit(solution)/shard_map/all_gather | solution.py:23
  147.8 0.2 reshape.143
  148.2 0.5 reshape_reshape.12
  148.9 3.3 fusion.3
  152.2 0.2 copy-done.1
  152.4 1.5 fusion.69
  153.9 1.4 fusion.63
  155.3 1.4 fusion.57
  156.7 1.4 fusion.51
  158.1 1.4 fusion.72
  159.5 1.1 broadcast_in_dim.54
  160.6 26.7 %all-to-all-start = ((bf16[8,1024,64]{1,2,0:T(8,128)(2,1)}), bf16[8,1024,64]{1,2,0:T(8,128)(2,1)S(1)}, u32[]{:S(2)}, u32[]{:S(2)}) async-start(bf16[8,1024,64]{1,2,0:T(8,128)(2,1)} %broadcast_in_dim.54), calls=%async_computation | async-start | bytes 2097152 | tf_op jit(solution)/shard_map/all_to_all | solution.py:33
  187.3 0.1 slice.27
  187.4 0.1 mul.90
  187.5 0.1 reshape_reshape.14
  187.6 14.7 %all-to-all-done = bf16[8,1024,64]{1,2,0:T(8,128)(2,1)S(1)} async-done(((bf16[8,1024,64]{1,2,0:T(8,128)(2,1)}), bf16[8,1024,64]{1,2,0:T(8,128)(2,1)S(1)}, u32[]{:S(2)}, u32[]{:S(2)}) %all-to-all-start) | async-done | bytes 1048608 | tf_op jit(solution)/shard_map/all_to_all | solution.py:33
  202.3 0.5 convolution_convert_fusion
  202.8 1.3 fusion.38
  204.1 0.1 slice.28
  204.2 0.1 mul.98
  204.2 0.1 slice_bitcast_fusion
  204.3 4.8 %copy.28 = bf16[4,4,128,1024]{3,2,1,0:T(8,128)(2,1)} copy(bf16[4,4,128,1024]{3,2,0,1:T(8,128)(2,1)} %bitcast.61) | data formatting | bytes 8388608 | tf_op jit(solution)/shard_map/transpose | solution.py:48
  209.1 18.8 %all-gather.24.cloned.1.call-done = bf16[16,1024,128]{2,1,0:T(8,128)(2,1)} async-done(((bf16[4,1024,128]{2,1,0:T(8,128)(2,1)}), bf16[16,1024,128]{2,1,0:T(8,128)(2,1)}) %all-gather.24.cloned.1.call-update) | async-done | bytes 4194320 | tf_op jit(solution)/shard_map/all_gather | solution.py:45
  227.9 4.5 %copy.29 = bf16[4,4,1024,128]{3,2,1,0:T(8,128)(2,1)} copy(bf16[4,4,1024,128]{3,2,0,1:T(8,128)(2,1)} %bitcast.62) | data formatting | bytes 8388608 | tf_op jit(solution)/shard_map/transpose | solution.py:48
  232.4 6.4 %copy.30 = bf16[1024,16,128]{0,2,1:T(8,128)(2,1)} copy(bf16[1024,16,128]{2,0,1:T(8,128)(2,1)} %bitcast.59) | data formatting | bytes 8388608 | tf_op jit(solution)/shard_map/transpose | solution.py:16
  238.8 29.7 %all-gather.14.cloned.1.call-done = bf16[1024,2048]{1,0:T(8,128)(2,1)} async-done(((bf16[1024,256]{1,0:T(8,128)(2,1)}), bf16[1024,2048]{1,0:T(8,128)(2,1)}) %all-gather.14.cloned.1.call-update) | async-done | bytes 4194320 | tf_op jit(solution)/shard_map/all_gather | solution.py:122
  268.6 3.1 fusion
  271.6 14.6 %multiply_convert_fusion = bf16[1024,2048]{1,0:T(8,128)(2,1)} fusion(bf16[1024,2048]{0,1:T(8,128)(2,1)} %bitcast.64, f32[2048]{0:T(1024)S(1)} %slice_bitcast_fusion, f32[1024]{0:T(1024)S(1)} %mul.98, bf16[2048,1024]{1,0:T(8,128)(2,1)} %bitcast.63, bf16[1024,2048]{1,0:T(8,128)(2,1)} %all-gather.14.cloned.1.call-done, f32[2048]{0:T(1024)S(1)} %copy-done.5, ...), kind=kOutput, calls=%fused_computation.11 | convolution fusion | flops 8606711808 | bytes 16801792 | tf_op jit(solution)/shard_map/dot_general | solution.py:126
  286.3 2.5 copy.37
  288.7 52.6 %all_to_all.10 = bf16[8,1024,256]{2,1,0:T(8,128)(2,1)S(1)} all-to-all(bf16[8,1024,256]{2,1,0:T(8,128)(2,1)S(1)} %bitcast.60), channel_id=1, replica_groups=mesh['rep'=2,'fs_0'=4,'fs_1'=4,'tp'=8] {'tp'}, dimensions={0} | all-to-all | bytes 8388608 | tf_op jit(solution)/shard_map/all_to_all | solution.py:64
  341.4 0.6 convert_reduce_fusion
  342.0 0.5 copy-done.2
  342.4 0.9 fusion.79
  (39 shorter events, 0.4 us)
Async XLA Ops:
  6.5 195.7 %copy-start = (bf16[4,128,128]{2,1,0:T(8,128)(2,1)S(1)}, bf16[4,128,128]{2,1,0:T(8,128)(2,1)}, u32[]{:S(2)}) copy-start(bf16[4,128,128]{2,1,0:T(8,128)(2,1)} %param.16) | copy-start | bytes 393220
  6.5 39.2 %all-gather.18.cloned.1.call-start = ((), (), s32[]{:S(2)}) async-start(), calls=%async_computation.4 | async-start | bytes 1310720 | tf_op jit(solution)/shard_map/all_gather | solution.py:45
  8.4 139.7 %all-gather.22.cloned.1.call-start = ((), (), s32[]{:S(2)}) async-start(), calls=%async_computation.6 | async-start | bytes 1310720 | tf_op jit(solution)/shard_map/all_gather | solution.py:45
  10.2 138.6 %all-gather.16.cloned.1.call-start = ((), (), s32[]{:S(2)}) async-start(), calls=%async_computation.3 | async-start | bytes 4718592 | tf_op jit(solution)/shard_map/all_gather | solution.py:107
  11.0 193.4 %all-gather.20.cloned.1.call-start = ((), (), s32[]{:S(2)}) async-start(), calls=%async_computation.5 | async-start | bytes 5242880 | tf_op jit(solution)/shard_map/all_gather | solution.py:45
  45.8 182.1 %all-gather.24.cloned.1.call-start = ((), (), s32[]{:S(2)}) async-start(), calls=%async_computation.7 | async-start | bytes 5242880 | tf_op jit(solution)/shard_map/all_gather | solution.py:45
  147.8 4.3 %copy-start.4 = (f32[2048]{0:T(1024)S(1)}, f32[2048]{0:T(1024)}, u32[]{:S(2)}) copy-start(f32[2048]{0:T(1024)} %param.13) | copy-start | bytes 24580
  148.9 3.5 %copy-start.1 = (bf16[1,1024,2048]{2,1,0:T(8,128)(2,1)S(1)}, bf16[1,1024,2048]{2,1,0:T(8,128)(2,1)}, u32[]{:S(2)}) copy-start(bf16[1,1024,2048]{2,1,0:T(8,128)(2,1)} %all-gather.16.cloned.1.call-done) | copy-start | bytes 12582916
  158.1 44.7 %copy-start.3 = (bf16[1,1024,256]{2,1,0:T(8,128)(2,1)S(1)}, bf16[1,1024,256]{2,1,0:T(8,128)(2,1)}, u32[]{:S(2)}) copy-start(bf16[1,1024,256]{2,1,0:T(8,128)(2,1)} %param.12) | copy-start | bytes 1572868
  160.6 41.7 %all-to-all-start = ((bf16[8,1024,64]{1,2,0:T(8,128)(2,1)}), bf16[8,1024,64]{1,2,0:T(8,128)(2,1)S(1)}, u32[]{:S(2)}, u32[]{:S(2)}) async-start(bf16[8,1024,64]{1,2,0:T(8,128)(2,1)} %broadcast_in_dim.54), calls=%async_computation | async-start | bytes 2097152 | tf_op jit(solution)/shard_map/all_to_all | solution.py:33
  187.3 81.3 %all-gather.14.cloned.1.call-start = ((), (), s32[]{:S(2)}) async-start(), calls=%async_computation.2 | async-start | bytes 4718592 | tf_op jit(solution)/shard_map/all_gather | solution.py:122
  238.8 32.8 %copy-start.5 = (f32[2048]{0:T(1024)S(1)}, f32[2048]{0:T(1024)}, u32[]{:S(2)}) copy-start(f32[2048]{0:T(1024)} %param.19) | copy-start | bytes 24580
  341.4 1.0 copy-start.2
Sparse Core Ops, SparseCore 0:
  9.1 36.5 all-gather.17
  47.5 33.1 all-gather.21
  82.6 37.5 all-gather.15
  121.8 54.8 all-gather.19
  178.4 49.4 all-gather.23
  229.6 38.9 all-gather.13
where the time goes:
time: 351 us; the launch traced here: 350 us
  blocking collectives  150 us (43%)
  waiting for transfers between devices  98.7 us (28%)
  starting transfers between devices  26.9 us (8%)
  matrix products  23.5 us (7%)
  local copies, waits for them, and re-layouts  23.1 us (7%)
  between operations  14.4 us (4%)
  other arithmetic  13.9 us (4%)
    unnamed x1, blocking collectives  64 us
    all_gather x4, waiting for transfers between devices, stacked_from(): parts = lax.all_gather(parts, axes[k])  53.5 us
    all_to_all x1, blocking collectives, sent_and_summed(): parts = lax.all_to_all(cut_along(array, dim, count), axis, 0, 0, tiled=True)  52.6 us
    all_gather x1, blocking collectives, gather_packed(): lines, at, finished = (lax.all_gather(ravelled, axis), 0, [])  33.1 us
    all_gather x1, waiting for transfers between devices, on_device(): mixed_full = lax.all_gather(mixed, 'tp', axis=1, tiled=True)  29.7 us
    all_to_all x1, starting transfers between devices, sent_to_all(): lax.all_to_all(jnp.broadcast_to(array[None], (count, *array.shape)), axis...  26.7 us
    all_to_all x1, waiting for transfers between devices, sent_to_all(): lax.all_to_all(jnp.broadcast_to(array[None], (count, *array.shape)), axis...  14.7 us
    dot_general x1, matrix products, on_device(): jnp.dot(hidden, whole_of(w_down.astype(jnp.bfloat16), FS, (0, 1), 1), pre...  14.6 us
  transfers between devices with their start and end apart: 7, of which 4 were waited for; matrix products, arithmetic and copies ran while one was open for 10% of the time, Pallas kernels for 0%

commit v1 on v0

--- a/solution.py
+++ b/solution.py
@@ -10,6 +10,22 @@
 REP_FS = ("rep", "fs_0", "fs_1")
 TP_FS = ("tp", "fs_0", "fs_1")
 epsilon = 0.25
+
+
+def collect_2(x, axis, dim):
+    ways, here, step = (lax.axis_size(axis), lax.axis_index(axis), x.shape[dim])
+    shape = [n * ways if d == dim else n for d, n in enumerate(x.shape)]
+    full = lax.dynamic_update_slice_in_dim(jnp.zeros(shape, x.dtype), x, here * step, axis=dim)
+    going_up = going_down = x
+    for far in range(1, ways // 2 + 1):
+        going_up = lax.ppermute(going_up, axis, [(d, (d + 1) % ways) for d in range(ways)])
+        full = lax.dynamic_update_slice_in_dim(full, going_up, (here - far) % ways * step, axis=dim)
+        if 2 * far < ways:
+            going_down = lax.ppermute(going_down, axis, [(d, (d - 1) % ways) for d in range(ways)])
+            full = lax.dynamic_update_slice_in_dim(
+                full, going_down, (here + far) % ways * step, axis=dim
+            )
+    return full
 
 
 def laid_out(parts, dim):
@@ -119,7 +135,7 @@
     grouped = grouped.reshape(length, PW).astype(jnp.bfloat16)
     branch = jnp.dot(grouped, out_whole, preferred_element_type=jnp.float32)
     mixed = (tokens.astype(jnp.float32) + branch * scale_out).astype(jnp.bfloat16)
-    mixed_full = lax.all_gather(mixed, "tp", axis=1, tiled=True)
+    mixed_full = collect_2(mixed, "tp", 1)
     ffn_in = rms_rows(mixed_full, ffn_gain)
     upward = fold_rows(ffn_in, whole_of(w_up.astype(jnp.bfloat16), FS, (0, 1), 0))
     hidden = jnp.square(jax.nn.relu(upward * scale_up)).astype(jnp.bfloat16)

time: 351 us -> 340 us (0.969)
  waiting for transfers between devices: 98.7 us -> 63.5 us
  starting transfers between devices: 26.9 us -> 36.3 us
  local copies, waits for them, and re-layouts: 23.1 us -> 31.9 us
  blocking collectives: 150 us -> 157 us
    all_gather x1 -> x0, waiting for transfers between devices: 29.7 us -> none  [on_device(): mixed_full = lax.all_gather(mixed, 'tp', axis=1, tiled=True)]
    all_gather x4, waiting for transfers between devices: 53.5 us -> 34.7 us  [stacked_from(): parts = lax.all_gather(parts, axes[k])]
    ppermute x0 -> x7, waiting for transfers between devices: none -> 13.5 us  [the longest x4 11.1 us: collect_2(): lax.ppermute(going_up, axis, [(d, (d + 1) % ways) for d in range(ways)])]
    ppermute x0 -> x7, starting transfers between devices: none -> 9.17 us  [the longest x4 6.11 us: collect_2(): lax.ppermute(going_up, axis, [(d, (d + 1) % ways) for d in range(ways)])]
    all_gather x1, blocking collectives: 33.1 us -> 39.1 us  [gather_packed(): lines, at, finished = (lax.all_gather(ravelled, axis), 0, [])]
    dynamic_update_slice x0 -> x7, local copies, waits for them, and re-layouts: none -> 5.92 us  [the longest x4 3.39 us: collect_2(): lax.dynamic_update_slice_in_dim(full, going_up, (here - far) % ways * ste...]
    all_to_all x1, blocking collectives: 52.6 us -> 57.6 us  [sent_and_summed(): parts = lax.all_to_all(cut_along(array, dim, count), axis, 0, 0, tiled=True)]
  transfers between devices with their start and end apart: 7 -> 13, of which waited for: 4 -> 6; matrix products, arithmetic and copies ran while one was open for 10% -> 13% of each run, Pallas kernels for 0% -> 0%
where the time goes in v1:
time: 340 us; the launch traced here: 339 us
  blocking collectives  157 us (46%)
  waiting for transfers between devices  63.5 us (19%)
  starting transfers between devices  36.3 us (11%)
  local copies, waits for them, and re-layouts  31.9 us (9%)
  matrix products  23.5 us (7%)
  between operations  14.1 us (4%)
  other arithmetic  12.6 us (4%)
    unnamed x1, blocking collectives  60.6 us
    all_to_all x1, blocking collectives, sent_and_summed(): parts = lax.all_to_all(cut_along(array, dim, count), axis, 0, 0, tiled=True)  57.6 us
    all_gather x1, blocking collectives, gather_packed(): lines, at, finished = (lax.all_gather(ravelled, axis), 0, [])  39.1 us
    all_gather x4, waiting for transfers between devices, stacked_from(): parts = lax.all_gather(parts, axes[k])  34.7 us
    all_to_all x1, starting transfers between devices, sent_to_all(): lax.all_to_all(jnp.broadcast_to(array[None], (count, *array.shape)), axis...  27 us
    dot_general x1, matrix products, on_device(): jnp.dot(hidden, whole_of(w_down.astype(jnp.bfloat16), FS, (0, 1), 1), pre...  14.7 us
    all_to_all x1, waiting for transfers between devices, sent_to_all(): lax.all_to_all(jnp.broadcast_to(array[None], (count, *array.shape)), axis...  14.5 us
    ppermute x4, waiting for transfers between devices, collect_2(): lax.ppermute(going_up, axis, [(d, (d + 1) % ways) for d in range(ways)])  11.1 us
  transfers between devices with their start and end apart: 13, of which 6 were waited for; matrix products, arithmetic and copies ran while one was open for 13% of the time, Pallas kernels for 0%

profile of v1, /device:TPU:1, one launch (start us, length us, event | category | flops | bytes accessed | tf_op | source)
XLA Modules:
  0.0 339.3 jit_solution(11022188930587272060)
XLA Ops:
  6.6 1.8 convert_element_type.118
  8.5 1.8 convert_element_type.116
  10.4 0.7 all-gather.13.cloned.1.call-update
  11.1 34.7 %all-gather.19.cloned.1.call-done = bf16[4096,128]{1,0:T(8,128)(2,1)} async-done(((bf16[1024,128]{1,0:T(8,128)(2,1)}), bf16[4096,128]{1,0:T(8,128)(2,1)}) %all-gather.19.cloned.1.call-update) | async-done | bytes 1048592 | tf_op jit(solution)/shard_map/all_gather | solution.py:61
  45.8 0.8 convert_element_type.100
  46.8 0.8 convert_bitcast_fusion
  47.6 39.1 %all-gather.1 = bf16[262144]{0:T(1024)(128)(2,1)S(1)} all-gather(bf16[16384]{0:T(1024)(128)(2,1)S(1)} %pad_maximum_fusion), channel_id=3, replica_groups=mesh['rep'=2,'fs_0'=4,'fs_1'=4,'tp'=8] {'fs_0','fs_1'}, dimensions={0}, use_global_device_ids=true | all-gather | bytes 557056 | tf_op jit(solution)/shard_map/all_gather | solution.py:39
  87.1 0.6 dynamic-slice
  88.6 60.6 %all-reduce = f32[3392]{0:T(1024)S(1)} all-reduce(f32[3392]{0:T(1024)S(1)} %maximum_dynamic-update-slice_fusion), channel_id=4, replica_groups=mesh['rep'=2,'fs_0'=4,'fs_1'=4,'tp'=8] {'fs_0','fs_1'}, use_global_device_ids=true, to_apply=%add | all-reduce | flops 3392 | bytes 27136
  149.4 0.5 reshape_reshape.12
  150.1 3.3 fusion.3
  153.7 1.5 fusion.69
  155.1 1.4 fusion.63
  156.5 1.4 fusion.57
  157.9 1.4 fusion.51
  159.3 1.4 fusion.72
  160.7 1.1 broadcast_in_dim.57
  161.9 27.0 %all-to-all-start = ((bf16[8,1024,64]{1,2,0:T(8,128)(2,1)}), bf16[8,1024,64]{1,2,0:T(8,128)(2,1)S(1)}, u32[]{:S(2)}, u32[]{:S(2)}) async-start(bf16[8,1024,64]{1,2,0:T(8,128)(2,1)} %broadcast_in_dim.57), calls=%async_computation | async-start | bytes 2097152 | tf_op jit(solution)/shard_map/all_to_all | solution.py:49
  189.3 14.5 %all-to-all-done = bf16[8,1024,64]{1,2,0:T(8,128)(2,1)S(1)} async-done(((bf16[8,1024,64]{1,2,0:T(8,128)(2,1)}), bf16[8,1024,64]{1,2,0:T(8,128)(2,1)S(1)}, u32[]{:S(2)}, u32[]{:S(2)}) %all-to-all-start) | async-done | bytes 1048608 | tf_op jit(solution)/shard_map/all_to_all | solution.py:49
  203.8 0.5 convolution_convert_fusion
  204.3 2.5 broadcast_in_dim.58
  206.8 1.3 constant_dynamic-update-slice_fusion.7
  208.1 1.1 collective-permute-start
  209.2 6.1 %collective-permute-done = bf16[1024,256]{0,1:T(8,128)(2,1)S(1)} collective-permute-done((bf16[1024,256]{0,1:T(8,128)(2,1)S(1)}, bf16[1024,256]{0,1:T(8,128)(2,1)S(1)}, u32[]{:S(2)}, u32[]{:S(2)}) %collective-permute-start) | collective-permute-done | bytes 524320 | tf_op jit(solution)/shard_map/ppermute | solution.py:21
  215.3 2.5 collective-permute-start.2
  217.8 0.4 collective-permute-done.1
  218.2 0.7 collective-permute-start.3
  218.9 5.0 %collective-permute-done.2 = bf16[1024,256]{0,1:T(8,128)(2,1)S(1)} collective-permute-done((bf16[1024,256]{0,1:T(8,128)(2,1)S(1)}, bf16[1024,256]{0,1:T(8,128)(2,1)S(1)}, u32[]{:S(2)}, u32[]{:S(2)}) %collective-permute-start.2) | collective-permute-done | bytes 524320 | tf_op jit(solution)/shard_map/ppermute | solution.py:21
  223.9 2.5 collective-permute-start.4
  226.6 4.6 %copy.36 = bf16[4,4,1024,128]{3,2,1,0:T(8,128)(2,1)} copy(bf16[4,4,1024,128]{3,2,0,1:T(8,128)(2,1)} %bitcast.61) | data formatting | bytes 8388608 | tf_op jit(solution)/shard_map/transpose | solution.py:64
  231.3 6.4 %copy.37 = bf16[1024,16,128]{0,2,1:T(8,128)(2,1)} copy(bf16[1024,16,128]{2,0,1:T(8,128)(2,1)} %bitcast.59) | data formatting | bytes 8388608 | tf_op jit(solution)/shard_map/transpose | solution.py:32
  237.7 4.8 %copy.35 = bf16[4,4,128,1024]{3,2,1,0:T(8,128)(2,1)} copy(bf16[4,4,128,1024]{3,2,0,1:T(8,128)(2,1)} %bitcast.62) | data formatting | bytes 8388608 | tf_op jit(solution)/shard_map/transpose | solution.py:64
  242.5 2.3 collective-permute-start.5
  244.8 0.9 constant_dynamic-update-slice_fusion.6
  245.7 0.8 constant_dynamic-update-slice_fusion.5
  246.5 0.8 constant_dynamic-update-slice_fusion.4
  247.4 0.9 constant_dynamic-update-slice_fusion.3
  248.2 0.8 constant_dynamic-update-slice_fusion.2
  249.1 2.0 collective-permute-done.5
  251.1 0.8 constant_dynamic-update-slice_fusion.1
  251.9 0.8 constant_dynamic-update-slice_fusion
  252.8 3.1 fusion
  255.9 14.7 %multiply_convert_fusion = bf16[1024,2048]{1,0:T(8,128)(2,1)} fusion(bf16[1024,2048]{0,1:T(8,128)(2,1)} %bitcast.63, f32[2048]{0:T(1024)S(1)} %slice_bitcast_fusion, f32[1024]{0:T(1024)S(1)} %mul.130, bf16[2048,1024]{1,0:T(8,128)(2,1)} %bitcast.64, bf16[1024,2048]{0,1:T(8,128)(2,1)} %constant_dynamic-update-slice_fusion, f32[2048]{0:T(1024)S(1)} %copy-done.8, ...), kind=kOutput, calls=%fused_computation.11 | convolution fusion | flops 8606711808 | bytes 16801792 | tf_op jit(solution)/shard_map/dot_general | solution.py:142
  270.6 2.5 copy.48
  273.0 57.6 %all_to_all.10 = bf16[8,1024,256]{2,1,0:T(8,128)(2,1)S(1)} all-to-all(bf16[8,1024,256]{2,1,0:T(8,128)(2,1)S(1)} %bitcast.60), channel_id=1, replica_groups=mesh['rep'=2,'fs_0'=4,'fs_1'=4,'tp'=8] {'tp'}, dimensions={0} | all-to-all | bytes 8388608 | tf_op jit(solution)/shard_map/all_to_all | solution.py:80
  330.7 0.6 convert_reduce_fusion
  331.2 0.3 copy.40
  331.7 1.0 copy.41
  (69 shorter events, 2.4 us)
Async XLA Ops:
  6.5 197.3 %copy-start = (bf16[4,128,128]{2,1,0:T(8,128)(2,1)S(1)}, bf16[4,128,128]{2,1,0:T(8,128)(2,1)}, u32[]{:S(2)}) copy-start(bf16[4,128,128]{2,1,0:T(8,128)(2,1)} %param.16) | copy-start | bytes 393220
  6.5 80.6 %copy-start.9 = (u32[256]{0:T(256)S(1)}, u32[256]{0:T(256)}, u32[]{:S(2)}) copy-start(u32[256]{0:T(256)} %constant.119) | copy-start | bytes 3076
  6.5 81.8 %copy-start.6 = (f32[4]{0:T(128)S(1)}, f32[4]{0:T(128)}, u32[]{:S(2)}) copy-start(f32[4]{0:T(128)} %param.15) | copy-start | bytes 52
  6.5 81.8 %copy-start.5 = (f32[16]{0:T(128)S(1)}, f32[16]{0:T(128)}, u32[]{:S(2)}) copy-start(f32[16]{0:T(128)} %param.18) | copy-start | bytes 196
  6.5 81.8 %copy-start.4 = (f32[64]{0:T(128)S(1)}, f32[64]{0:T(128)}, u32[]{:S(2)}) copy-start(f32[64]{0:T(128)} %param.21) | copy-start | bytes 772
  6.5 81.8 %copy-start.3 = (f32[128]{0:T(128)S(1)}, f32[128]{0:T(128)}, u32[]{:S(2)}) copy-start(f32[128]{0:T(128)} %param.23) | copy-start | bytes 1540
  6.6 39.2 %all-gather.19.cloned.1.call-start = ((), (), s32[]{:S(2)}) async-start(), calls=%async_computation.5 | async-start | bytes 1310720 | tf_op jit(solution)/shard_map/all_gather | solution.py:61
  8.4 78.6 %all-gather.15.cloned.1.call-start = ((), (), s32[]{:S(2)}) async-start(), calls=%async_computation.3 | async-start | bytes 1310720 | tf_op jit(solution)/shard_map/all_gather | solution.py:61
  10.3 139.8 %all-gather.13.cloned.1.call-start = ((), (), s32[]{:S(2)}) async-start(), calls=%async_computation.2 | async-start | bytes 4718592 | tf_op jit(solution)/shard_map/all_gather | solution.py:123
  11.1 215.6 %all-gather.21.cloned.1.call-start = ((), (), s32[]{:S(2)}) async-start(), calls=%async_computation.6 | async-start | bytes 5242880 | tf_op jit(solution)/shard_map/all_gather | solution.py:61
  45.8 191.9 %all-gather.17.cloned.1.call-start = ((), (), s32[]{:S(2)}) async-start(), calls=%async_computation.4 | async-start | bytes 5242880 | tf_op jit(solution)/shard_map/all_gather | solution.py:61
  86.8 66.7 %copy-start.7 = (f32[2048]{0:T(1024)S(1)}, f32[2048]{0:T(1024)}, u32[]{:S(2)}) copy-start(f32[2048]{0:T(1024)} %param.13) | copy-start | bytes 24580
  150.1 3.5 %copy-start.1 = (bf16[1,1024,2048]{2,1,0:T(8,128)(2,1)S(1)}, bf16[1,1024,2048]{2,1,0:T(8,128)(2,1)}, u32[]{:S(2)}) copy-start(bf16[1,1024,2048]{2,1,0:T(8,128)(2,1)} %all-gather.13.cloned.1.call-done) | copy-start | bytes 12582916
  159.3 29.6 %copy-start.2 = (bf16[1,1024,256]{2,1,0:T(8,128)(2,1)S(1)}, bf16[1,1024,256]{2,1,0:T(8,128)(2,1)}, u32[]{:S(2)}) copy-start(bf16[1,1024,256]{2,1,0:T(8,128)(2,1)} %param.12) | copy-start | bytes 1572868
  161.9 41.9 %all-to-all-start = ((bf16[8,1024,64]{1,2,0:T(8,128)(2,1)}), bf16[8,1024,64]{1,2,0:T(8,128)(2,1)S(1)}, u32[]{:S(2)}, u32[]{:S(2)}) async-start(bf16[8,1024,64]{1,2,0:T(8,128)(2,1)} %broadcast_in_dim.57), calls=%async_computation | async-start | bytes 2097152 | tf_op jit(solution)/shard_map/all_to_all | solution.py:49
  208.1 7.3 %collective-permute-start = (bf16[1024,256]{0,1:T(8,128)(2,1)S(1)}, bf16[1024,256]{0,1:T(8,128)(2,1)S(1)}, u32[]{:S(2)}, u32[]{:S(2)}) collective-permute-start(bf16[1024,256]{0,1:T(8,128)(2,1)S(1)} %get-tuple-element.8), channel_id=1, source_target_pairs={{0,1},{1,2},{2,3},{3,4},{4,5},{5,6},{6,7},{7,0},{8,9},{9,10},{10,1... | collective-permute-start | bytes 1572872 | tf_op jit(solution)/shard_map/ppermute | solution.py:21
  209.2 9.0 %collective-permute-start.1 = (bf16[1024,256]{0,1:T(8,128)(2,1)S(1)}, bf16[1024,256]{0,1:T(8,128)(2,1)S(1)}, u32[]{:S(2)}, u32[]{:S(2)}) collective-permute-start(bf16[1024,256]{0,1:T(8,128)(2,1)S(1)} %get-tuple-element.8), channel_id=1, source_target_pairs={{0,7},{1,0},{2,1},{3,2},{4,3},{5,4},{6,5},{7,6},{8,15},{9,8},{10,9... | collective-permute-start | bytes 1572872 | tf_op jit(solution)/shard_map/ppermute | solution.py:24
  215.3 8.6 %collective-permute-start.2 = (bf16[1024,256]{0,1:T(8,128)(2,1)S(1)}, bf16[1024,256]{0,1:T(8,128)(2,1)S(1)}, u32[]{:S(2)}, u32[]{:S(2)}) collective-permute-start(bf16[1024,256]{0,1:T(8,128)(2,1)S(1)} %collective-permute-done), channel_id=1, source_target_pairs={{0,1},{1,2},{2,3},{3,4},{4,5},{5,6},{6,7},{7,0},{8,9},{9,10},{10,1... | collective-permute-start | bytes 1572872 | tf_op jit(solution)/shard_map/ppermute | solution.py:21
  218.2 24.3 %collective-permute-start.3 = (bf16[1024,256]{0,1:T(8,128)(2,1)S(1)}, bf16[1024,256]{0,1:T(8,128)(2,1)S(1)}, u32[]{:S(2)}, u32[]{:S(2)}) collective-permute-start(bf16[1024,256]{0,1:T(8,128)(2,1)S(1)} %collective-permute-done.1), channel_id=1, source_target_pairs={{0,7},{1,0},{2,1},{3,2},{4,3},{5,4},{6,5},{7,6},{8,15},{9,8},{10,9... | collective-permute-start | bytes 1572872 | tf_op jit(solution)/shard_map/ppermute | solution.py:24
  223.9 21.8 %collective-permute-start.4 = (bf16[1024,256]{0,1:T(8,128)(2,1)S(1)}, bf16[1024,256]{0,1:T(8,128)(2,1)S(1)}, u32[]{:S(2)}, u32[]{:S(2)}) collective-permute-start(bf16[1024,256]{0,1:T(8,128)(2,1)S(1)} %collective-permute-done.2), channel_id=1, source_target_pairs={{0,1},{1,2},{2,3},{3,4},{4,5},{5,6},{6,7},{7,0},{8,9},{9,10},{10,1... | collective-permute-start | bytes 1572872 | tf_op jit(solution)/shard_map/ppermute | solution.py:21
  242.5 8.6 %collective-permute-start.5 = (bf16[1024,256]{0,1:T(8,128)(2,1)S(1)}, bf16[1024,256]{0,1:T(8,128)(2,1)S(1)}, u32[]{:S(2)}, u32[]{:S(2)}) collective-permute-start(bf16[1024,256]{0,1:T(8,128)(2,1)S(1)} %collective-permute-done.3), channel_id=1, source_target_pairs={{0,7},{1,0},{2,1},{3,2},{4,3},{5,4},{6,5},{7,6},{8,15},{9,8},{10,9... | collective-permute-start | bytes 1572872 | tf_op jit(solution)/shard_map/ppermute | solution.py:24
  245.7 6.2 %collective-permute-start.6 = (bf16[1024,256]{0,1:T(8,128)(2,1)S(1)}, bf16[1024,256]{0,1:T(8,128)(2,1)S(1)}, u32[]{:S(2)}, u32[]{:S(2)}) collective-permute-start(bf16[1024,256]{0,1:T(8,128)(2,1)S(1)} %collective-permute-done.4), channel_id=1, source_target_pairs={{0,1},{1,2},{2,3},{3,4},{4,5},{5,6},{6,7},{7,0},{8,9},{9,10},{10,1... | collective-permute-start | bytes 1572872 | tf_op jit(solution)/shard_map/ppermute | solution.py:21
  247.4 8.5 %copy-start.8 = (f32[2048]{0:T(1024)S(1)}, f32[2048]{0:T(1024)}, u32[]{:S(2)}) copy-start(f32[2048]{0:T(1024)} %param.19) | copy-start | bytes 24580
Sparse Core Ops, SparseCore 0:
  9.2 36.5 all-gather.18
  47.6 34.5 all-gather.14
  84.0 38.2 all-gather.12
  124.0 51.7 all-gather.20
  177.4 50.8 all-gather.16
